TPU v7x, 32 devices: a whole 2x2x4 slice. The times are simulated.
32 devices in a mesh: sp: 8 (over z, y), tp: 4 (over x, core).
Axes of the slice: x: 2, y: 2, z: 4, core: 2. Of those that a mesh axis runs over, the one named last changes fastest.
Arguments:
- tokens: bfloat16 [4096, 2048], P(('sp', 'tp')), may hold values from -6 to 6
- norm_gain: float32 [2048], replicated, may hold values from 0.25 to 5
- w_query_one: bfloat16 [2048, 512], P(None, 'tp'), may hold values from -0.21875 to 0.21875
- w_query_two: bfloat16 [2048, 512], P(None, 'tp'), may hold values from -0.21875 to 0.21875
- w_key_one: bfloat16 [2048, 512], P(None, 'tp'), may hold values from -0.125 to 0.125
- w_key_two: bfloat16 [2048, 512], P(None, 'tp'), may hold values from -0.125 to 0.125
- w_value: bfloat16 [2048, 1024], P(None, 'tp'), may hold values from -0.125 to 0.125
- mix_lambda: float32 [8], P('tp'), may hold values from 0.3 to 0.8
- head_gain: float32 [128], replicated, may hold values from 0.1 to 1.9
- w_ret_query: bfloat16 [2048, 512], P(None, 'tp'), may hold values from -0.125 to 0.125
- w_ret_key: bfloat16 [2048, 512], P(None, 'tp'), may hold values from -0.125 to 0.125
- w_ret_value: bfloat16 [2048, 1024], P(None, 'tp'), may hold values from -0.125 to 0.125
- retain_log: float32 [8, 4096], P('tp', 'sp'), may hold values from -1 to 0
- init_state: float32 [8, 64, 128], P('tp'), may hold values from -144 to 144
- w_out_diff: bfloat16 [1024, 2048], P('tp'), may hold values from -0.125 to 0.125
- w_out_ret: bfloat16 [1024, 2048], P('tp'), may hold values from -0.125 to 0.125
Outputs:
- mixed: bfloat16 [4096, 2048], P(('sp', 'tp'))
All inputs are finite; a program needn't handle non-finite values.
Results may differ from a plain program's by a relative error of at most 0.015.
The roundings to bfloat16 on the way count: a program that leaves them out, or rounds other values in their place, can miss the bound.
Values may be sent and summed in bfloat16 or wider, within the bound.
A program may use at most 128 MiB of HBM per device.

v0:
```python
import math

import jax
import jax.numpy as jnp
from jax import lax
from jax.sharding import PartitionSpec as P

BLOCK = 256


NORM_EPS = 1e-06
HEAD_EPS = 1e-05
DIFF_SCALE = 0.8
HIGHEST = lax.Precision.HIGHEST


def prefix(x, axis, join, neutral):
    place = lax.axis_index(axis)
    gathered = jax.tree.map(
        lambda a, kind: lax.all_gather(a.astype(kind), axis), x, (jnp.bfloat16, jnp.bfloat16)
    )
    state = jax.tree.map(lambda a, e: jnp.zeros_like(a) + jnp.asarray(e, a.dtype), x, neutral)

    def one(turn, state):
        return join(
            state,
            jax.tree.map(
                lambda a, own: lax.dynamic_index_in_dim(a, turn, 0, False).astype(own.dtype),
                gathered,
                x,
            ),
        )

    return lax.fori_loop(0, place, one, state)


def head_norm(values):
    return values * lax.rsqrt(jnp.mean(values * values, axis=-1, keepdims=True) + HEAD_EPS)


def soft_update(running, query, keys, values, allowed):
    peak_old, denominator, weighted = running
    scores = jnp.einsum(
        "qhd,khd->hqk", query, keys, preferred_element_type=jnp.float32
    ) * query.shape[-1] ** (-0.5)
    scores = jnp.where(allowed[None], scores, -jnp.inf)
    peak_new = jnp.maximum(peak_old, jnp.max(scores, axis=-1))
    offset = jnp.where(jnp.isinf(peak_new), 0.0, peak_new)
    rescale = jnp.exp(peak_old - offset)
    shifted = jnp.exp(scores - offset[..., None])
    denominator = denominator * rescale + jnp.sum(shifted, axis=-1)
    weighted = weighted * rescale[..., None] + jnp.einsum(
        "hqk,khe->hqe", shifted.astype(jnp.bfloat16), values, preferred_element_type=jnp.float32
    )
    return (peak_new, denominator, weighted)


def on_device(
    tokens,
    norm_gain,
    w_query_one,
    w_query_two,
    w_key_one,
    w_key_two,
    w_value,
    mix_lambda,
    head_gain,
    w_ret_query,
    w_ret_key,
    w_ret_value,
    retain_log,
    init_state,
    w_out_diff,
    w_out_ret,
):
    key_width = w_query_one.shape[1]
    diff_heads = mix_lambda.shape[0]
    head_dim = key_width // diff_heads
    val_dim = head_gain.shape[0]
    value_width = w_value.shape[1]
    ret_heads = init_state.shape[0]
    ret_width = w_ret_query.shape[1]
    floats = tokens.astype(jnp.float32)
    normed = (
        floats * lax.rsqrt(jnp.mean(floats * floats, axis=-1, keepdims=True) + NORM_EPS) * norm_gain
    ).astype(jnp.bfloat16)
    weights = (
        w_query_one,
        w_query_two,
        w_key_one,
        w_key_two,
        w_value,
        w_ret_query,
        w_ret_key,
        w_ret_value,
    )
    portion = lax.all_gather(normed, "tp", axis=0, tiled=True)
    projected = jnp.concatenate(
        [
            jnp.dot(portion, weight, preferred_element_type=jnp.float32).astype(jnp.bfloat16)
            for weight in weights
        ],
        axis=1,
    )
    row_count = projected.shape[0]
    query_one = projected[:, :key_width].reshape(row_count, diff_heads, head_dim)
    query_two = projected[:, key_width : 2 * key_width].reshape(row_count, diff_heads, head_dim)
    key_pack = projected[:, 2 * key_width : 4 * key_width + value_width]
    ret_begin = 4 * key_width + value_width
    ret_query = projected[:, ret_begin : ret_begin + ret_width]
    ret_key = projected[:, ret_begin + ret_width : ret_begin + 2 * ret_width]
    ret_value = projected[:, ret_begin + 2 * ret_width :]
    nblocks = row_count // BLOCK

    def split_blocks(data, size):
        return data.reshape(nblocks, BLOCK, ret_heads, size).transpose(0, 2, 1, 3)

    block_query = split_blocks(ret_query, head_dim)
    block_key = split_blocks(ret_key, head_dim)
    block_value = split_blocks(ret_value, val_dim)
    log_blocks = retain_log.reshape(ret_heads, nblocks, BLOCK).transpose(1, 0, 2)
    sequence_index = jnp.arange(BLOCK, dtype=jnp.int32)
    causal = sequence_index[:, None] >= sequence_index[None, :]

    def ret_step(memory, inputs):
        query, keys, values, logs = inputs
        cumulative = jnp.cumsum(logs, axis=-1)
        gap_log = jnp.where(causal[None], cumulative[:, :, None] - cumulative[:, None, :], -jnp.inf)
        raw = jnp.einsum("hqd,hkd->hqk", query, keys, preferred_element_type=jnp.float32)
        decayed = (raw * head_dim ** (-0.5) * jnp.exp(gap_log)).astype(jnp.bfloat16)
        result = jnp.einsum("hqk,hke->hqe", decayed, values, preferred_element_type=jnp.float32)
        result = result + jnp.einsum(
            "hqd,hde->hqe",
            query.astype(jnp.float32) * jnp.exp(cumulative)[:, :, None],
            memory,
            precision=HIGHEST,
        )
        last_log = cumulative[:, -1:]
        key_scaled = (
            keys.astype(jnp.float32)
            * head_dim ** (-0.5)
            * jnp.exp(last_log - cumulative)[:, :, None]
        ).astype(jnp.bfloat16)
        memory = jnp.exp(last_log)[:, :, None] * memory + jnp.einsum(
            "hkd,hke->hde", key_scaled, values, preferred_element_type=jnp.float32
        )
        return (memory, result)

    zero_state = jnp.zeros((ret_heads, head_dim, val_dim), jnp.float32)
    local_state, local_out = lax.scan(
        ret_step, zero_state, (block_query, block_key, block_value, log_blocks)
    )
    span_log = jnp.sum(retain_log, axis=1)

    def chain_states(first_part, second_part):
        return (
            first_part[0] + second_part[0],
            first_part[1] * jnp.exp(second_part[0])[:, None, None] + second_part[1],
        )

    before_log, before_state = prefix(
        (span_log, local_state), "sp", chain_states, (jnp.zeros_like(span_log), zero_state)
    )
    carried = before_state + jnp.exp(before_log)[:, None, None] * init_state
    span_cumulative = jnp.cumsum(retain_log, axis=1)
    scaled_query = (
        ret_query.astype(jnp.float32).reshape(row_count, ret_heads, head_dim)
        * jnp.exp(span_cumulative).T[:, :, None]
    )
    ret_heads_out = local_out.transpose(1, 0, 2, 3).reshape(
        ret_heads, row_count, val_dim
    ) + jnp.einsum("thd,hde->hte", scaled_query, carried, precision=HIGHEST)
    ret_out = (
        head_norm(ret_heads_out)
        .transpose(1, 0, 2)
        .reshape(row_count, ret_heads * val_dim)
        .astype(jnp.bfloat16)
    )
    place = lax.axis_index("sp")
    query_pos = place * row_count + jnp.arange(row_count, dtype=jnp.int32)
    last_pos = place * row_count + row_count - 1

    def attend(running, key_block, begin_at):
        key_count = key_block.shape[0]
        keys_one = key_block[:, :key_width].reshape(key_count, diff_heads, head_dim)
        keys_two = key_block[:, key_width : 2 * key_width].reshape(key_count, diff_heads, head_dim)
        values = key_block[:, 2 * key_width :].reshape(key_count, diff_heads, val_dim)
        allowed = query_pos[:, None] >= (begin_at + jnp.arange(key_count, dtype=jnp.int32))[None, :]
        return (
            soft_update(running[0], query_one, keys_one, values, allowed),
            soft_update(running[1], query_two, keys_two, values, allowed),
        )

    empty_map = (
        jnp.full((diff_heads, row_count), -jnp.inf, jnp.float32),
        jnp.zeros((diff_heads, row_count), jnp.float32),
        jnp.zeros((diff_heads, row_count, val_dim), jnp.float32),
    )
    portion = lax.all_gather(key_pack, "sp", axis=0, tiled=True)
    key_count = portion.shape[0]
    stride = math.gcd(key_count, 512)

    def one_block(number, inner_state):
        first_pos = number * stride
        key_block = lax.dynamic_slice_in_dim(portion, number * stride, stride, 0)
        return lax.cond(
            first_pos <= last_pos,
            lambda kept: attend(kept, key_block, first_pos),
            lambda kept: kept,
            inner_state,
        )

    softmax_maps = lax.fori_loop(0, key_count // stride, one_block, (empty_map, empty_map))
    first_map, second_map = softmax_maps
    mixed_heads = (
        first_map[2] / first_map[1][..., None]
        - mix_lambda[:, None, None] * second_map[2] / second_map[1][..., None]
    )
    diff_out = (
        (head_norm(mixed_heads) * head_gain * DIFF_SCALE)
        .transpose(1, 0, 2)
        .reshape(row_count, diff_heads * val_dim)
        .astype(jnp.bfloat16)
    )
    return lax.psum_scatter(
        (
            jnp.dot(diff_out, w_out_diff, preferred_element_type=jnp.float32)
            + jnp.dot(ret_out, w_out_ret, preferred_element_type=jnp.float32)
        ).astype(jnp.bfloat16),
        "tp",
        scatter_dimension=0,
        tiled=True,
    )


def solution(mesh):
    in_specs = (
        P(("sp", "tp"), None),
        P(),
        P(None, "tp"),
        P(None, "tp"),
        P(None, "tp"),
        P(None, "tp"),
        P(None, "tp"),
        P("tp"),
        P(),
        P(None, "tp"),
        P(None, "tp"),
        P(None, "tp"),
        P("tp", "sp"),
        P("tp", None, None),
        P("tp", None),
        P("tp", None),
    )
    out_specs = P(("sp", "tp"), None)
    return jax.shard_map(
        on_device, mesh=mesh, in_specs=in_specs, out_specs=out_specs, check_vma=False
    )
```

profile of v0, /device:TPU:24, one launch (start us, length us, event | category | flops | bytes accessed | tf_op | source)
XLA Modules:
  0.0 261.5 jit_solution(5012526148714268753)
XLA Ops:
  11.6 16.8 %all-reduce = bf16[16]{0:T(256)(128)(2,1)S(1)} all-reduce(bf16[16]{0:T(256)(128)(2,1)S(1)} %dynamic-update-slice), channel_id=2, replica_groups=mesh['sp'=8,'tp'=4] {'sp'}, use_global_device_ids=true, to_apply=%add | all-reduce | flops 16 | bytes 64
  30.8 2.9 %all-gather.5.cloned.1.call-done = bf16[512,2048]{1,0:T(8,128)(2,1)} async-done(((bf16[128,2048]{1,0:T(8,128)(2,1)}), bf16[512,2048]{1,0:T(8,128)(2,1)}) %all-gather.5.cloned.1.call-update) | async-done | bytes 2097168 | tf_op jit(solution)/shard_map/all_gather | solution.py:97
  33.6 2.8 %convolution_convert_fusion.1 = bf16[512,256]{0,1:T(8,128)(2,1)S(1)} fusion(bf16[512,2048]{1,0:T(8,128)(2,1)} %all-gather.5.cloned.1.call-done, bf16[2048,256]{1,0:T(8,128)(2,1)} %param.30), kind=kOutput, calls=%fused_computation.83 | convolution fusion | flops 537001984 | bytes 3407872 | tf_op jit(solution)/shard_map/dot_general | solution.py:100
  42.7 2.6 %convolution_convert_fusion = bf16[512,256]{1,0:T(8,128)(2,1)} fusion(bf16[512,2048]{1,0:T(8,128)(2,1)S(1)} %copy-done.2, bf16[2048,256]{1,0:T(8,128)(2,1)} %param.35), kind=kOutput, calls=%fused_computation.82 | convolution fusion | flops 537001984 | bytes 3407872 | tf_op jit(solution)/shard_map/dot_general | solution.py:100
  51.4 14.2 %while.51 = (s32[]{:T(128)}, f32[2,64,128]{2,1,0:T(8,128)S(1)}, f32[2,2,256,128]{3,2,1,0:T(8,128)}, f32[2,2,256]{2,1,0:T(2,128)S(1)}, bf16[2,2,256,64]{2,3,1,0:T...) while((s32[]{:T(128)}, f32[2,64,128]{2,1,0:T(8,128)S(1)}, ...), condition=%wide.region_13.14_spmd.clone, body=%wide.region_10.13_spmd.clone.sunk | while | flops 110134280 | bytes 1677136 | solution.py:150
  65.6 36.4 %all-gather.1 = bf16[16,64,128]{2,1,0:T(8,128)(2,1)} all-gather(bf16[2,64,128]{2,1,0:T(8,128)(2,1)S(1)} %convert_element_type.128), channel_id=3, replica_groups=mesh['sp'=8,'tp'=4] {'sp'}, dimensions={0}, use_global_device_ids=true | all-gather | bytes 294912 | tf_op jit(solution)/shard_map/all_gather | solution.py:20
  102.1 9.3 %while.49 = (s32[]{:T(128)}, f32[2]{0:T(128)S(1)}, f32[2,64,128]{2,1,0:T(8,128)S(1)}, s32[]{:T(128)}, bf16[8,2]{1,0:T(8,128)(2,1)}, /*index=5*/bf16[8,2,64,128]{3,2,1,0:T(8,128)(2,1)}, s32[]{:T(128)}, s32[]{:T(128)}, s32[]{:T(128)}) while((s32[]{:T(128)}, f32[2]{0:T(128)S(1)}, f32[2,64,128]{2,1,0:T(8,128)S(1)}, s32[]{:T(128)}, ...), condition=%wide.region_18.19_spmd, body=%wide.region_17.18_spmd.sunk | while | flops 49161 | bytes 164011 | solution.py:34
  122.3 83.8 %while.50 = (s32[]{:T(128)}, f32[2,512]{1,0:T(2,128)S(1)}, f32[2,512]{1,0:T(2,128)S(1)}, f32[2,512,128]{2,1,0:T(8,128)}, f32[2,512]{1,0:T(2,128)S(1)}, /*index=5...) while((s32[]{:T(128)}, f32[2,512]{1,0:T(2,128)S(1)}, ...), condition=%wide.region_8.9_spmd.clone, body=%wide.region_1.8_spmd.clone.sunk | while | flops 410797056 | bytes 26628588 | solution.py:213
  122.3 12.0 %conditional.3 = ((f32[2,512]{1,0:T(2,128)S(1)}, f32[2,512]{1,0:T(2,128)S(1)}, f32[2,512,128]{2,1,0:T(8,128)}, f32[2,512]{1,0:T(2,128)S(1)}, f32[2,512]{1,0:T(2,128)S(1)}, /*index=5*/f32[2,512,128]{2,1,0:T(8,128)})) conditional(s32[]{:T(128)} %convert_element_type.180, (f32[2,512]{1,0:T(2,128)S(1)}, f32[2,512]{1,0:T(2,128)S(1)}, ...), branch_computations={%region_2.2_spmd, %region_3.7_spmd} | conditional | flops 410797056 | bytes 26626238 | solution.py:206
  128.4 3.1 %convolution_add_fusion = f32[2,512,128]{2,1,0:T(8,128)} fusion(bf16[512,2,128]{0,2,1:T(8,128)(2,1)S(1)} %bitcast.146, f32[2,512,512]{1,2,0:T(8,128)} %copy-done.1, f32[2,512]{1,0:T(2,128)S(1)} %get-tuple-element.549, f32[2,512,128]{2,1,0:T(8,128)} %get-tuple-element.368, f32[2,512]{1,0:T(2,128)S(1)} %get-tuple-element.548), kind=kOutput, calls=%fused_computation.10 | convolution fusion | flops 135528448 | bytes 3416064 | tf_op jit(solution)/shard_map/while/body/eval_jaxpr/cond/branch_1_fun/hqk,khe->hqe/dot_general | solution.py:52
  134.3 12.0 %conditional.3 = ((f32[2,512]{1,0:T(2,128)S(1)}, f32[2,512]{1,0:T(2,128)S(1)}, f32[2,512,128]{2,1,0:T(8,128)}, f32[2,512]{1,0:T(2,128)S(1)}, f32[2,512]{1,0:T(2,128)S(1)}, /*index=5*/f32[2,512,128]{2,1,0:T(8,128)})) conditional(s32[]{:T(128)} %convert_element_type.180, (f32[2,512]{1,0:T(2,128)S(1)}, f32[2,512]{1,0:T(2,128)S(1)}, ...), branch_computations={%region_2.2_spmd, %region_3.7_spmd} | conditional | flops 410797056 | bytes 26626238 | solution.py:206
  140.4 3.1 %convolution_add_fusion = f32[2,512,128]{2,1,0:T(8,128)} fusion(bf16[512,2,128]{0,2,1:T(8,128)(2,1)S(1)} %bitcast.146, f32[2,512,512]{1,2,0:T(8,128)} %copy-done.1, f32[2,512]{1,0:T(2,128)S(1)} %get-tuple-element.549, f32[2,512,128]{2,1,0:T(8,128)} %get-tuple-element.368, f32[2,512]{1,0:T(2,128)S(1)} %get-tuple-element.548), kind=kOutput, calls=%fused_computation.10 | convolution fusion | flops 135528448 | bytes 3416064 | tf_op jit(solution)/shard_map/while/body/eval_jaxpr/cond/branch_1_fun/hqk,khe->hqe/dot_general | solution.py:52
  143.8 2.4 convolution_add_fusion.1
  146.3 12.0 %conditional.3 = ((f32[2,512]{1,0:T(2,128)S(1)}, f32[2,512]{1,0:T(2,128)S(1)}, f32[2,512,128]{2,1,0:T(8,128)}, f32[2,512]{1,0:T(2,128)S(1)}, f32[2,512]{1,0:T(2,128)S(1)}, /*index=5*/f32[2,512,128]{2,1,0:T(8,128)})) conditional(s32[]{:T(128)} %convert_element_type.180, (f32[2,512]{1,0:T(2,128)S(1)}, f32[2,512]{1,0:T(2,128)S(1)}, ...), branch_computations={%region_2.2_spmd, %region_3.7_spmd} | conditional | flops 410797056 | bytes 26626238 | solution.py:206
  152.3 3.1 %convolution_add_fusion = f32[2,512,128]{2,1,0:T(8,128)} fusion(bf16[512,2,128]{0,2,1:T(8,128)(2,1)S(1)} %bitcast.146, f32[2,512,512]{1,2,0:T(8,128)} %copy-done.1, f32[2,512]{1,0:T(2,128)S(1)} %get-tuple-element.549, f32[2,512,128]{2,1,0:T(8,128)} %get-tuple-element.368, f32[2,512]{1,0:T(2,128)S(1)} %get-tuple-element.548), kind=kOutput, calls=%fused_computation.10 | convolution fusion | flops 135528448 | bytes 3416064 | tf_op jit(solution)/shard_map/while/body/eval_jaxpr/cond/branch_1_fun/hqk,khe->hqe/dot_general | solution.py:52
  158.2 12.0 %conditional.3 = ((f32[2,512]{1,0:T(2,128)S(1)}, f32[2,512]{1,0:T(2,128)S(1)}, f32[2,512,128]{2,1,0:T(8,128)}, f32[2,512]{1,0:T(2,128)S(1)}, f32[2,512]{1,0:T(2,128)S(1)}, /*index=5*/f32[2,512,128]{2,1,0:T(8,128)})) conditional(s32[]{:T(128)} %convert_element_type.180, (f32[2,512]{1,0:T(2,128)S(1)}, f32[2,512]{1,0:T(2,128)S(1)}, ...), branch_computations={%region_2.2_spmd, %region_3.7_spmd} | conditional | flops 410797056 | bytes 26626238 | solution.py:206
  164.3 3.1 %convolution_add_fusion = f32[2,512,128]{2,1,0:T(8,128)} fusion(bf16[512,2,128]{0,2,1:T(8,128)(2,1)S(1)} %bitcast.146, f32[2,512,512]{1,2,0:T(8,128)} %copy-done.1, f32[2,512]{1,0:T(2,128)S(1)} %get-tuple-element.549, f32[2,512,128]{2,1,0:T(8,128)} %get-tuple-element.368, f32[2,512]{1,0:T(2,128)S(1)} %get-tuple-element.548), kind=kOutput, calls=%fused_computation.10 | convolution fusion | flops 135528448 | bytes 3416064 | tf_op jit(solution)/shard_map/while/body/eval_jaxpr/cond/branch_1_fun/hqk,khe->hqe/dot_general | solution.py:52
  170.2 12.0 %conditional.3 = ((f32[2,512]{1,0:T(2,128)S(1)}, f32[2,512]{1,0:T(2,128)S(1)}, f32[2,512,128]{2,1,0:T(8,128)}, f32[2,512]{1,0:T(2,128)S(1)}, f32[2,512]{1,0:T(2,128)S(1)}, /*index=5*/f32[2,512,128]{2,1,0:T(8,128)})) conditional(s32[]{:T(128)} %convert_element_type.180, (f32[2,512]{1,0:T(2,128)S(1)}, f32[2,512]{1,0:T(2,128)S(1)}, ...), branch_computations={%region_2.2_spmd, %region_3.7_spmd} | conditional | flops 410797056 | bytes 26626238 | solution.py:206
  176.2 3.1 %convolution_add_fusion = f32[2,512,128]{2,1,0:T(8,128)} fusion(bf16[512,2,128]{0,2,1:T(8,128)(2,1)S(1)} %bitcast.146, f32[2,512,512]{1,2,0:T(8,128)} %copy-done.1, f32[2,512]{1,0:T(2,128)S(1)} %get-tuple-element.549, f32[2,512,128]{2,1,0:T(8,128)} %get-tuple-element.368, f32[2,512]{1,0:T(2,128)S(1)} %get-tuple-element.548), kind=kOutput, calls=%fused_computation.10 | convolution fusion | flops 135528448 | bytes 3416064 | tf_op jit(solution)/shard_map/while/body/eval_jaxpr/cond/branch_1_fun/hqk,khe->hqe/dot_general | solution.py:52
  182.1 12.0 %conditional.3 = ((f32[2,512]{1,0:T(2,128)S(1)}, f32[2,512]{1,0:T(2,128)S(1)}, f32[2,512,128]{2,1,0:T(8,128)}, f32[2,512]{1,0:T(2,128)S(1)}, f32[2,512]{1,0:T(2,128)S(1)}, /*index=5*/f32[2,512,128]{2,1,0:T(8,128)})) conditional(s32[]{:T(128)} %convert_element_type.180, (f32[2,512]{1,0:T(2,128)S(1)}, f32[2,512]{1,0:T(2,128)S(1)}, ...), branch_computations={%region_2.2_spmd, %region_3.7_spmd} | conditional | flops 410797056 | bytes 26626238 | solution.py:206
  188.2 3.1 %convolution_add_fusion = f32[2,512,128]{2,1,0:T(8,128)} fusion(bf16[512,2,128]{0,2,1:T(8,128)(2,1)S(1)} %bitcast.146, f32[2,512,512]{1,2,0:T(8,128)} %copy-done.1, f32[2,512]{1,0:T(2,128)S(1)} %get-tuple-element.549, f32[2,512,128]{2,1,0:T(8,128)} %get-tuple-element.368, f32[2,512]{1,0:T(2,128)S(1)} %get-tuple-element.548), kind=kOutput, calls=%fused_computation.10 | convolution fusion | flops 135528448 | bytes 3416064 | tf_op jit(solution)/shard_map/while/body/eval_jaxpr/cond/branch_1_fun/hqk,khe->hqe/dot_general | solution.py:52
  194.1 12.0 %conditional.3 = ((f32[2,512]{1,0:T(2,128)S(1)}, f32[2,512]{1,0:T(2,128)S(1)}, f32[2,512,128]{2,1,0:T(8,128)}, f32[2,512]{1,0:T(2,128)S(1)}, f32[2,512]{1,0:T(2,128)S(1)}, /*index=5*/f32[2,512,128]{2,1,0:T(8,128)})) conditional(s32[]{:T(128)} %convert_element_type.180, (f32[2,512]{1,0:T(2,128)S(1)}, f32[2,512]{1,0:T(2,128)S(1)}, ...), branch_computations={%region_2.2_spmd, %region_3.7_spmd} | conditional | flops 410797056 | bytes 26626238 | solution.py:206
  200.2 3.1 %convolution_add_fusion = f32[2,512,128]{2,1,0:T(8,128)} fusion(bf16[512,2,128]{0,2,1:T(8,128)(2,1)S(1)} %bitcast.146, f32[2,512,512]{1,2,0:T(8,128)} %copy-done.1, f32[2,512]{1,0:T(2,128)S(1)} %get-tuple-element.549, f32[2,512,128]{2,1,0:T(8,128)} %get-tuple-element.368, f32[2,512]{1,0:T(2,128)S(1)} %get-tuple-element.548), kind=kOutput, calls=%fused_computation.10 | convolution fusion | flops 135528448 | bytes 3416064 | tf_op jit(solution)/shard_map/while/body/eval_jaxpr/cond/branch_1_fun/hqk,khe->hqe/dot_general | solution.py:52
  212.3 42.7 %reduce-scatter.2.cloned.1.call-done = bf16[128,2048]{1,0:T(8,128)(2,1)} async-done(((bf16[512,2048]{1,0:T(8,128)(2,1)}), bf16[128,2048]{1,0:T(8,128)(2,1)}) %reduce-scatter.2.cloned.1.call-update) | async-done | bytes 524304 | tf_op jit(solution)/shard_map/reduce_scatter | solution.py:225
  (274 shorter events, 118.3 us)
Async XLA Ops:
  6.5 202.4 %copy-start = (bf16[256,2048]{1,0:T(8,128)(2,1)S(1)}, bf16[256,2048]{1,0:T(8,128)(2,1)}, u32[]{:S(2)}) copy-start(bf16[256,2048]{1,0:T(8,128)(2,1)} %param.38) | copy-start | bytes 3145732
  6.5 3.5 %copy-start.16 = (u32[32]{0:T(128)S(1)}, u32[32]{0:T(128)}, u32[]{:S(2)}) copy-start(u32[32]{0:T(128)} %constant.133) | copy-start | bytes 388
  6.5 4.7 %copy-start.10 = (f32[2,512]{1,0:T(2,128)S(1)}, f32[2,512]{1,0:T(2,128)}, u32[]{:S(2)}) copy-start(f32[2,512]{1,0:T(2,128)} %param.36) | copy-start | bytes 12292
  6.5 27.1 %all-gather.5.cloned.1.call-start = ((), (), s32[]{:S(2)}) async-start(), calls=%async_computation.1 | async-start | bytes 2621440 | tf_op jit(solution)/shard_map/all_gather | solution.py:97
  9.9 110.7 %all-gather.7.cloned.1.call-start = ((), (), s32[]{:S(2)}) async-start(), calls=%async_computation.2 | async-start | bytes 4718592 | tf_op jit(solution)/shard_map/all_gather | solution.py:199
  33.6 2.8 %copy-start.2 = (bf16[512,2048]{1,0:T(8,128)(2,1)S(1)}, bf16[512,2048]{1,0:T(8,128)(2,1)}, u32[]{:S(2)}) copy-start(bf16[512,2048]{1,0:T(8,128)(2,1)} %all-gather.5.cloned.1.call-done) | copy-start | bytes 6291460
  36.4 1.9 copy-start.6
  40.0 214.9 %reduce-scatter.2.cloned.1.call-start = ((), (), s32[]{:S(2)}) async-start(), calls=%async_computation.3 | async-start | bytes 2621440 | tf_op jit(solution)/shard_map/reduce_scatter | solution.py:225
  42.0 3.4 %copy-start.3 = (bf16[512,128]{0,1:T(8,128)(2,1)}, bf16[512,128]{0,1:T(8,128)(2,1)S(1)}, u32[]{:S(2)}) copy-start(bf16[512,128]{0,1:T(8,128)(2,1)S(1)} %convolution_convert_fusion.2) | copy-start | bytes 393220
  65.6 50.1 %copy-start.4 = (bf16[512,128]{0,1:T(8,128)(2,1)S(1)}, bf16[512,128]{0,1:T(8,128)(2,1)}, u32[]{:S(2)}) copy-start(bf16[512,128]{0,1:T(8,128)(2,1)} %copy-done.3) | copy-start | bytes 393220
  65.6 50.1 %copy-start.11 = (f32[2,64,128]{2,1,0:T(8,128)S(1)}, f32[2,64,128]{2,1,0:T(8,128)}, u32[]{:S(2)}) copy-start(f32[2,64,128]{2,1,0:T(8,128)} %param.37) | copy-start | bytes 196612
  65.6 50.1 %copy-start.12 = (f32[1,2,4,128]{3,1,2,0:T(2,128)S(1)}, f32[1,2,4,128]{3,1,2,0:T(2,128)}, u32[]{:S(2)}) copy-start(f32[1,2,4,128]{3,1,2,0:T(2,128)} %copy.66) | copy-start | bytes 12292
  115.7 1.9 copy-start.7
  117.5 1.6 copy-start.8
  122.3 2.8 %copy-start.9 = (bf16[512,2,64]{0,2,1:T(8,128)(2,1)S(1)}, bf16[512,2,64]{0,2,1:T(8,128)(2,1)}, u32[]{:S(2)}) copy-start(bf16[512,2,64]{0,2,1:T(8,128)(2,1)} %get-tuple-element.366) | copy-start | bytes 393220 | tf_op jit(solution)/shard_map/while/body/eval_jaxpr/cond
  125.8 1.3 copy-start.1
  134.3 2.8 %copy-start.9 = (bf16[512,2,64]{0,2,1:T(8,128)(2,1)S(1)}, bf16[512,2,64]{0,2,1:T(8,128)(2,1)}, u32[]{:S(2)}) copy-start(bf16[512,2,64]{0,2,1:T(8,128)(2,1)} %get-tuple-element.366) | copy-start | bytes 393220 | tf_op jit(solution)/shard_map/while/body/eval_jaxpr/cond
  146.3 2.8 %copy-start.9 = (bf16[512,2,64]{0,2,1:T(8,128)(2,1)S(1)}, bf16[512,2,64]{0,2,1:T(8,128)(2,1)}, u32[]{:S(2)}) copy-start(bf16[512,2,64]{0,2,1:T(8,128)(2,1)} %get-tuple-element.366) | copy-start | bytes 393220 | tf_op jit(solution)/shard_map/while/body/eval_jaxpr/cond
  158.2 2.8 %copy-start.9 = (bf16[512,2,64]{0,2,1:T(8,128)(2,1)S(1)}, bf16[512,2,64]{0,2,1:T(8,128)(2,1)}, u32[]{:S(2)}) copy-start(bf16[512,2,64]{0,2,1:T(8,128)(2,1)} %get-tuple-element.366) | copy-start | bytes 393220 | tf_op jit(solution)/shard_map/while/body/eval_jaxpr/cond
  170.2 2.8 %copy-start.9 = (bf16[512,2,64]{0,2,1:T(8,128)(2,1)S(1)}, bf16[512,2,64]{0,2,1:T(8,128)(2,1)}, u32[]{:S(2)}) copy-start(bf16[512,2,64]{0,2,1:T(8,128)(2,1)} %get-tuple-element.366) | copy-start | bytes 393220 | tf_op jit(solution)/shard_map/while/body/eval_jaxpr/cond
  182.1 2.8 %copy-start.9 = (bf16[512,2,64]{0,2,1:T(8,128)(2,1)S(1)}, bf16[512,2,64]{0,2,1:T(8,128)(2,1)}, u32[]{:S(2)}) copy-start(bf16[512,2,64]{0,2,1:T(8,128)(2,1)} %get-tuple-element.366) | copy-start | bytes 393220 | tf_op jit(solution)/shard_map/while/body/eval_jaxpr/cond
  194.1 2.8 %copy-start.9 = (bf16[512,2,64]{0,2,1:T(8,128)(2,1)S(1)}, bf16[512,2,64]{0,2,1:T(8,128)(2,1)}, u32[]{:S(2)}) copy-start(bf16[512,2,64]{0,2,1:T(8,128)(2,1)} %get-tuple-element.366) | copy-start | bytes 393220 | tf_op jit(solution)/shard_map/while/body/eval_jaxpr/cond
  206.1 2.5 copy-start.14
  206.1 2.7 %copy-start.15 = (f32[128]{0:T(128)S(1)}, f32[128]{0:T(128)}, u32[]{:S(2)}) copy-start(f32[128]{0:T(128)} %param.32) | copy-start | bytes 1540
  (9 other events, 10.3 us)
Sparse Core Ops, SparseCore 0:
  10.0 23.5 all-gather.4
  40.2 76.3 all-gather.6
  212.4 42.5 reduce-scatter.1
where the time goes:
time: 266 us; the launch traced here: 262 us
  matrix products  82.5 us (31%)
  blocking collectives  53.3 us (20%)
  waiting for transfers between devices  45.6 us (17%)
  local copies, waits for them, and re-layouts  42.4 us (16%)
  other arithmetic  22.7 us (9%)
  between operations  14.1 us (5%)
    reduce_scatter x1, waiting for transfers between devices, on_device(): lax.psum_scatter((jnp.dot(diff_out, w_out_diff, preferred_element_type=jn...  42.7 us
    dot_general x14, matrix products, soft_update(): jnp.einsum('hqk,khe->hqe', shifted.astype(jnp.bfloat16), values, preferre...  38.8 us
    all_gather x1, blocking collectives, prefix(): lax.all_gather(a.astype(kind), axis)  36.4 us
    unnamed x1, blocking collectives  16.8 us
    dot_general x14, matrix products, soft_update(): jnp.einsum('qhd,khd->hqk', query, keys, preferred_element_type=jnp.float32)  15 us
    dot_general x8, matrix products, on_device(): jnp.dot(portion, weight, preferred_element_type=jnp.float32)  14.8 us
    cond x42, local copies, waits for them, and re-layouts  9.16 us
    slice x7, local copies, waits for them, and re-layouts, attend(): key_block[:, key_width:2 * key_width]  7.19 us
  transfers between devices with their start and end apart: 3, of which 2 were waited for; matrix products, arithmetic and copies ran while one was open for 18% of the time, Pallas kernels for 0%

commit v1 on v0

v1 whole, which is shorter than its diff:
```python
import functools

import jax
import jax.numpy as jnp
from jax import lax
from jax.experimental import pallas as pl
from jax.experimental.pallas import tpu as pltpu
from jax.sharding import PartitionSpec as P

BLOCK = 256
NORM_EPS = 1e-06
HEAD_EPS = 1e-05
DIFF_SCALE = 0.8
HIGHEST = lax.Precision.HIGHEST
MESH = pl.DeviceIdType.MESH
F32 = jnp.float32
BF16 = jnp.bfloat16
VMEM_LIMIT = 60 * 1024 * 1024


def remote(src, dst, send, recv, where):
    return pltpu.make_async_remote_copy(
        src_ref=src, dst_ref=dst, send_sem=send, recv_sem=recv,
        device_id=where, device_id_type=MESH,
    )


def head_norm(values):
    return values * lax.rsqrt(jnp.mean(values * values, axis=-1, keepdims=True) + HEAD_EPS)


def nn(a, b, **kw):
    return lax.dot_general(a, b, (((1,), (0,)), ((), ())), preferred_element_type=F32, **kw)


def nt(a, b):
    return lax.dot_general(a, b, (((1,), (1,)), ((), ())), preferred_element_type=F32)


def tn(a, b):
    return lax.dot_general(a, b, (((0,), (0,)), ((), ())), preferred_element_type=F32)


def project_kernel(ntp, widths, tokens_ref, gain_ref, *refs):
    nw = len(widths)
    w_refs = refs[:nw]
    q_ref, kv_ref, r_ref = refs[nw : nw + 3]
    gat, wbuf, wsem, pair_send, cross_send, recv = refs[nw + 3 :]
    me = lax.axis_index("tp")
    core = lax.rem(me, 2)
    chip = me // 2
    nchip = ntp // 2
    pair = me + 1 - 2 * core
    rows = tokens_ref.shape[0]
    barrier = pltpu.get_barrier_semaphore()
    pl.semaphore_signal(barrier, inc=1, device_id={"tp": pair}, device_id_type=MESH)
    for d in range(1, nchip):
        there = lax.rem(chip + d, nchip) * 2 + core
        pl.semaphore_signal(barrier, inc=1, device_id={"tp": there}, device_id_type=MESH)
    loads = []
    at = 0
    for n, width in enumerate(widths):
        loads.append(pltpu.make_async_copy(w_refs[n], wbuf.at[:, at : at + width], wsem.at[n]))
        loads[-1].start()
        at += width
    floats = tokens_ref[...].astype(F32)
    gat[me] = (
        floats * lax.rsqrt(jnp.mean(floats * floats, axis=-1, keepdims=True) + NORM_EPS) * gain_ref[...]
    ).astype(BF16)
    pl.semaphore_wait(barrier, nchip)
    crosses = []
    for d in range(1, nchip):
        there = lax.rem(chip + d, nchip) * 2 + core
        for half in range(2):
            part = pl.ds(half * (rows // 2), rows // 2)
            copy = remote(gat.at[me, part], gat.at[me, part], cross_send.at[d, half],
                          recv.at[me, half], {"tp": there})
            copy.start()
            crosses.append(copy)
    pairs = []

    def to_pair(which, half):
        part = pl.ds(half * (rows // 2), rows // 2)
        copy = remote(gat.at[which, part], gat.at[which, part], pair_send.at[which // 2, half],
                      recv.at[which, half], {"tp": pair})
        copy.start()
        pairs.append(copy)

    def landed(which, half):
        part = pl.ds(half * (rows // 2), rows // 2)
        remote(gat.at[which, part], gat.at[which, part], pair_send.at[which // 2, half],
               recv.at[which, half], {"tp": pair}).wait_recv()

    outs = (q_ref, kv_ref, r_ref)
    total = sum(widths)
    kinds = [(0, 2), (2, 5), (5, 8)]

    def project(which_chip):
        both = gat[pl.ds(which_chip * 2, 2)].reshape(2 * rows, gat.shape[2])
        where = pl.ds(pl.multiple_of(which_chip * 2 * rows, 2 * rows), 2 * rows)
        for out, (lo, hi) in zip(outs, kinds):
            start = sum(widths[:lo])
            span = sum(widths[lo:hi])
            cut = 256 if span % 256 == 0 else span
            for c in range(0, span, cut):
                out[where, c : c + cut] = nn(both, wbuf[:, start + c : start + c + cut]).astype(BF16)

    for half in range(2):
        to_pair(me, half)
    for load in loads:
        load.wait()
    for half in range(2):
        landed(pair, half)
    project(chip)
    for d in range(1, nchip):
        other = lax.rem(chip + nchip - d, nchip)
        for half in range(2):
            landed(other * 2 + core, half)
            to_pair(other * 2 + core, half)
        for half in range(2):
            landed(other * 2 + 1 - core, half)
        project(other)
    for copy in crosses + pairs:
        copy.wait_send()


def mix_kernel(nsp, heads, rheads, lam_ref, gain_ref, log_ref, init_ref, q_ref, r_ref, kv_hbm,
               out_ref, kvs, sts, qs, peak, den, acc, rmid, upd, ownsem, sem_z, sem_y, sem_rk,
               sem_zs, sem_ys, sem_rs):
    me = lax.axis_index("sp")
    b = lax.rem(me, 2)
    p = me // 2
    npair = nsp // 2
    rows, qw = q_ref.shape
    kw = qw // 2
    hd = kw // heads
    val = gain_ref.shape[1]
    up = {"sp": lax.rem(me + 2, nsp)}
    side = {"sp": me + 1 - 2 * b}
    own = pltpu.make_async_copy(kv_hbm, kvs.at[me], ownsem)
    own.start()
    barrier = pltpu.get_barrier_semaphore()
    pl.semaphore_signal(barrier, inc=1, device_id=side, device_id_type=MESH)

    @pl.when(p > 0)
    def _():
        pl.semaphore_signal(barrier, inc=1, device_id={"sp": lax.rem(me + nsp - 2, nsp)}, device_id_type=MESH)

    @pl.when(p < npair - 1)
    def _():
        pl.semaphore_signal(barrier, inc=1, device_id=up, device_id_type=MESH)

    pl.semaphore_wait(barrier, 1 + jnp.minimum(p, 1) + jnp.minimum(npair - 1 - p, 1))

    def kv_copy(i, j, sem, where):
        return remote(kvs.at[j], kvs.at[j], sem.at[i], sem_rk.at[j], where)

    def st_copy(i, j, sem, where):
        return remote(sts.at[j], sts.at[j], sem.at[i], sem_rs.at[j], where)

    own.wait()
    first_up = p < npair - 1

    @pl.when(first_up)
    def _():
        kv_copy(0, me, sem_z, up).start()

    @pl.when(b == 0)
    def _():
        kv_copy(0, me, sem_y, side).start()

    blk = BLOCK
    nblk = rows // blk
    vw = rheads * val
    rkw = rheads * hd
    tt = lax.broadcasted_iota(jnp.int32, (blk, blk), 0)
    uu = lax.broadcasted_iota(jnp.int32, (blk, blk), 1)
    lane = lax.broadcasted_iota(jnp.int32, (blk, rkw), 1)
    srow = lax.broadcasted_iota(jnp.int32, (rkw, val), 0)
    decays = []
    span_state = jnp.zeros((rkw, val), F32)
    span_logs = []
    for h in range(rheads):
        mine = (lane >= h * hd) & (lane < (h + 1) * hd)
        keep = (srow >= h * hd) & (srow < (h + 1) * hd)
        state = jnp.zeros((rkw, val), F32)
        log_all = jnp.zeros((1, 1), F32)
        for n in range(nblk):
            at = slice(n * blk, (n + 1) * blk)
            row = log_ref[h : h + 1, at]
            full = jnp.broadcast_to(row, (blk, blk))
            c_col = jnp.sum(jnp.where(uu <= tt, full, 0.0), axis=1, keepdims=True)
            l_col = jnp.sum(jnp.where(uu == tt, full, 0.0), axis=1, keepdims=True)
            c_row = jnp.sum(jnp.where(tt <= uu, l_col, 0.0), axis=0, keepdims=True)
            last = c_col[blk - 1 : blk, :]
            query = jnp.where(mine, r_ref[at, :rkw].astype(F32), 0.0)
            keys = r_ref[at, rkw : 2 * rkw]
            values = r_ref[at, 2 * rkw + h * val : 2 * rkw + (h + 1) * val]
            raw = nt(query.astype(BF16), keys)
            gap = jnp.where(uu <= tt, c_col - c_row, -jnp.inf)
            g = (raw * hd ** (-0.5) * jnp.exp(gap)).astype(BF16)
            rmid[h, at, :] = nn(g, values)
            kd = (keys.astype(F32) * hd ** (-0.5) * jnp.exp(last - c_col)).astype(BF16)
            new = jnp.where(keep, tn(kd, values), 0.0)
            upd[h, n] = new
            state = jnp.exp(last) * state + new
            log_all = log_all + last
            decays.append((c_col, last))
        span_state = span_state + state
        span_logs.append(log_all)
    sts[me, :rkw, :] = span_state.astype(BF16)
    for h in range(rheads):
        wide = jnp.broadcast_to(span_logs[h], (16, val))
        hi = wide.astype(BF16)
        sts[me, rkw + 32 * h : rkw + 32 * h + 16, :] = hi
        sts[me, rkw + 32 * h + 16 : rkw + 32 * h + 32, :] = (wide - hi.astype(F32)).astype(BF16)

    qlane = lax.broadcasted_iota(jnp.int32, (rows, kw), 1)
    for m in range(2):
        piece = q_ref[:, m * kw : (m + 1) * kw].astype(F32) * hd ** (-0.5)
        for h in range(heads):
            mine = (qlane >= h * hd) & (qlane < (h + 1) * hd)
            qs[m * heads + h] = jnp.where(mine, piece, 0.0).astype(BF16)
    qb = min(rows, 256)

    def attend(j, diagonal):
        @pl.loop(0, 2 * heads)
        def _(mh):
            m = mh // heads
            h = lax.rem(mh, heads)
            kcol = pl.ds(pl.multiple_of(m * kw, kw), kw)
            vcol = pl.ds(pl.multiple_of(2 * kw + h * val, val), val)
            for n in range(rows // qb):
                at = slice(n * qb, (n + 1) * qb)
                count = (n + 1) * qb if diagonal else rows
                scores = nt(qs[mh, at, :], kvs[j, :count, kcol])
                if diagonal:
                    ti = lax.broadcasted_iota(jnp.int32, (qb, count), 0) + n * qb
                    ui = lax.broadcasted_iota(jnp.int32, (qb, count), 1)
                    scores = jnp.where(ui <= ti, scores, -jnp.inf)
                top = jnp.max(scores, axis=1, keepdims=True)
                if not diagonal:
                    old = peak[mh, at, :]
                    top = jnp.maximum(old, top)
                e = jnp.exp(scores - top[:, :1])
                part = e[:, :128]
                for c in range(128, count, 128):
                    part = part + e[:, c : c + 128]
                weighted = nn(e.astype(BF16), kvs[j, :count, vcol])
                if diagonal:
                    peak[mh, at, :] = jnp.broadcast_to(top, (qb, 128))
                    den[mh, at, :] = part
                    acc[mh, at, :] = weighted
                else:
                    rescale = jnp.exp(old - top)
                    peak[mh, at, :] = top
                    den[mh, at, :] = den[mh, at, :] * rescale + part
                    acc[mh, at, :] = acc[mh, at, :] * rescale[:, :1] + weighted

    attend(me, True)

    @pl.when(first_up)
    def _():
        st_copy(0, me, sem_zs, up).start()

    @pl.when(b == 0)
    def _():
        st_copy(0, me, sem_ys, side).start()

    @pl.loop(1, npair + 1)
    def _(i):
        jz = 2 * (p - i) + b
        jy = 2 * (p - i + 1) + 1 - b

        @pl.when(i <= p)
        def _():
            kv_copy(i, jz, sem_z, up).wait_recv()

            @pl.when(first_up)
            def _():
                kv_copy(i, jz, sem_z, up).start()

            kv_copy(i, jz, sem_y, side).start()
            st_copy(i, jz, sem_zs, up).wait_recv()

            @pl.when(first_up)
            def _():
                st_copy(i, jz, sem_zs, up).start()

            st_copy(i, jz, sem_ys, side).start()
            attend(jz, False)

        @pl.when((i - 1 <= p) & ((b == 1) | (i > 1)))
        def _():
            kv_copy(i, jy, sem_y, side).wait_recv()
            st_copy(i, jy, sem_ys, side).wait_recv()
            attend(jy, False)

    for h in range(heads):
        pieces = []
        for m in range(2):
            mh = m * heads + h
            total = jnp.sum(den[mh], axis=1, keepdims=True)
            pieces.append(acc[mh] / total)
        mixed = pieces[0] - lam_ref[h] * pieces[1]
        out_ref[:, h * val : (h + 1) * val] = (head_norm(mixed) * gain_ref[...] * DIFF_SCALE).astype(BF16)

    first = []
    for h in range(rheads):
        parts = [jnp.zeros((hd, val), F32)] * h + [init_ref[h]] + [jnp.zeros((hd, val), F32)] * (rheads - 1 - h)
        first.append(jnp.concatenate(parts, axis=0) if rheads > 1 else parts[0])

    def join(j, states):
        out = []
        for h in range(rheads):
            keep = (srow >= h * hd) & (srow < (h + 1) * hd)
            base = rkw + 32 * h
            log = sts[j, base : base + 16, :].astype(F32) + sts[j, base + 16 : base + 32, :].astype(F32)
            piece = jnp.where(keep, sts[j, :rkw, :].astype(F32), 0.0)
            out.append(jnp.exp(log[:1, :]) * states[h] + piece)
        return tuple(out)

    carried = lax.fori_loop(0, me, join, tuple(first))
    for h in range(rheads):
        state = carried[h]
        for n in range(nblk):
            at = slice(n * blk, (n + 1) * blk)
            c_col, last = decays[h * nblk + n]
            query = r_ref[at, :rkw].astype(F32) * jnp.exp(c_col)
            result = rmid[h, at, :] + nn(query, state, precision=HIGHEST)
            if n + 1 < nblk:
                state = jnp.exp(last) * state + upd[h, n]
            out_ref[at, heads * val + h * val : heads * val + (h + 1) * val] = head_norm(result).astype(BF16)

    @pl.loop(0, npair)
    def _(i):
        j = 2 * (p - i) + b

        @pl.when((i <= p) & first_up)
        def _():
            kv_copy(i, j, sem_z, up).wait_send()
            st_copy(i, j, sem_zs, up).wait_send()

        @pl.when((i <= p) & ((i > 0) | (b == 0)))
        def _():
            kv_copy(i, j, sem_y, side).wait_send()
            st_copy(i, j, sem_ys, side).wait_send()


def merge_kernel(ntp, mix_ref, wd_ref, wr_ref, out_ref, wbuf, mine, sent, from_pair, from_chip,
                 wsem, pair_send, pair_recv, chip_send, chip_recv):
    me = lax.axis_index("tp")
    core = lax.rem(me, 2)
    chip = me // 2
    nchip = ntp // 2
    pair = {"tp": me + 1 - 2 * core}
    rows, width = out_ref.shape
    depth = wd_ref.shape[0]
    cut = mine.shape[2]
    pieces = width // cut
    barrier = pltpu.get_barrier_semaphore()
    pl.semaphore_signal(barrier, inc=1, device_id=pair, device_id_type=MESH)
    for d in range(1, nchip):
        there = lax.rem(chip + d, nchip) * 2 + core
        pl.semaphore_signal(barrier, inc=1, device_id={"tp": there}, device_id_type=MESH)
    loads = [
        pltpu.make_async_copy(wd_ref, wbuf.at[:depth], wsem.at[0]),
        pltpu.make_async_copy(wr_ref, wbuf.at[depth:], wsem.at[1]),
    ]
    for load in loads:
        load.start()
    for load in loads:
        load.wait()
    pl.semaphore_wait(barrier, nchip)

    def partial(owner, n):
        part = mix_ref[pl.ds(pl.multiple_of(owner * rows, rows), rows), :]
        return nn(part, wbuf[:, n * cut : (n + 1) * cut])

    def pair_copy(d, n):
        return remote(mine.at[d * pieces + n], from_pair.at[d * pieces + n], pair_send.at[d, n],
                      pair_recv.at[d, n], pair)

    def chip_copy(d, n):
        there = lax.rem(chip + d, nchip) * 2 + core
        return remote(sent.at[d * pieces + n], from_chip.at[d * pieces + n], chip_send.at[d, n],
                      chip_recv.at[d, n], {"tp": there})

    order = list(range(1, nchip)) + [0]
    for d in order:
        target = lax.rem(chip + d, nchip) * 2
        for n in range(pieces):
            mine[d * pieces + n] = partial(target + 1 - core, n).astype(BF16)
            pair_copy(d, n).start()
        if d:
            for n in range(pieces):
                ours = partial(target + core, n)
                pair_copy(d, n).wait_recv()
                sent[d * pieces + n] = (ours + from_pair[d * pieces + n].astype(F32)).astype(BF16)
                chip_copy(d, n).start()
    for n in range(pieces):
        total = partial(me, n)
        pair_copy(0, n).wait_recv()
        total = total + from_pair[n].astype(F32)
        for d in range(1, nchip):
            chip_copy(d, n).wait_recv()
            total = total + from_chip[d * pieces + n].astype(F32)
        out_ref[:, n * cut : (n + 1) * cut] = total.astype(BF16)
    for d in order:
        for n in range(pieces):
            pair_copy(d, n).wait_send()
            if d:
                chip_copy(d, n).wait_send()


VMEM = pl.BlockSpec(memory_space=pltpu.VMEM)
ANY = pl.BlockSpec(memory_space=pl.ANY)
SMEM = pl.BlockSpec(memory_space=pltpu.SMEM)
DMA = pltpu.SemaphoreType.DMA


def params(number):
    return pltpu.CompilerParams(
        collective_id=number, has_side_effects=True, vmem_limit_bytes=VMEM_LIMIT
    )


def on_device(nsp, ntp, tokens, norm_gain, w_query_one, w_query_two, w_key_one, w_key_two, w_value,
              mix_lambda, head_gain, w_ret_query, w_ret_key, w_ret_value, retain_log, init_state,
              w_out_diff, w_out_ret):
    weights = (w_query_one, w_query_two, w_key_one, w_key_two, w_value, w_ret_query, w_ret_key, w_ret_value)
    widths = tuple(w.shape[1] for w in weights)
    own_rows, model = tokens.shape
    rows = own_rows * ntp
    nchip = ntp // 2
    q, kv, r = pl.pallas_call(
        functools.partial(project_kernel, ntp, widths),
        out_shape=[
            jax.ShapeDtypeStruct((rows, sum(widths[:2])), BF16),
            jax.ShapeDtypeStruct((rows, sum(widths[2:5])), BF16),
            jax.ShapeDtypeStruct((rows, sum(widths[5:])), BF16),
        ],
        in_specs=[VMEM, VMEM] + [ANY] * len(weights),
        out_specs=[VMEM] * 3,
        scratch_shapes=[
            pltpu.VMEM((ntp, own_rows, model), BF16),
            pltpu.VMEM((model, sum(widths)), BF16),
            DMA((len(weights),)),
            DMA((nchip, 2)),
            DMA((nchip, 2)),
            DMA((ntp, 2)),
        ],
        compiler_params=params(0),
        name="project",
    )(tokens, norm_gain[None, :], *weights)
    heads = mix_lambda.shape[0]
    rheads, hd, val = init_state.shape
    kw = widths[2]
    npair = nsp // 2
    mixers = pl.pallas_call(
        functools.partial(mix_kernel, nsp, heads, rheads),
        out_shape=jax.ShapeDtypeStruct((rows, (heads + rheads) * val), BF16),
        in_specs=[SMEM, VMEM, VMEM, VMEM, VMEM, VMEM, ANY],
        out_specs=VMEM,
        scratch_shapes=[
            pltpu.VMEM((nsp, rows, kv.shape[1]), BF16),
            pltpu.VMEM((nsp, rheads * hd + 32 * rheads, val), BF16),
            pltpu.VMEM((2 * heads, rows, kw), BF16),
            pltpu.VMEM((2 * heads, rows, 128), F32),
            pltpu.VMEM((2 * heads, rows, 128), F32),
            pltpu.VMEM((2 * heads, rows, val), F32),
            pltpu.VMEM((rheads, rows, val), F32),
            pltpu.VMEM((rheads, rows // BLOCK, rheads * hd, val), F32),
            DMA,
            DMA((npair + 1,)),
            DMA((npair + 1,)),
            DMA((nsp,)),
            DMA((npair + 1,)),
            DMA((npair + 1,)),
            DMA((nsp,)),
        ],
        compiler_params=params(1),
        name="mixers",
    )(mix_lambda, head_gain[None, :], retain_log, init_state, q, r, kv)
    width = w_out_diff.shape[1]
    pieces = 4
    cut = width // pieces
    return pl.pallas_call(
        functools.partial(merge_kernel, ntp),
        out_shape=jax.ShapeDtypeStruct((own_rows, width), BF16),
        in_specs=[VMEM, ANY, ANY],
        out_specs=VMEM,
        scratch_shapes=[
            pltpu.VMEM((w_out_diff.shape[0] + w_out_ret.shape[0], width), BF16),
            pltpu.VMEM((nchip * pieces, own_rows, cut), BF16),
            pltpu.VMEM((nchip * pieces, own_rows, cut), BF16),
            pltpu.VMEM((nchip * pieces, own_rows, cut), BF16),
            pltpu.VMEM((nchip * pieces, own_rows, cut), BF16),
            DMA((2,)),
            DMA((nchip, pieces)),
            DMA((nchip, pieces)),
            DMA((nchip, pieces)),
            DMA((nchip, pieces)),
        ],
        compiler_params=params(2),
        name="merge",
    )(mixers, w_out_diff, w_out_ret)


def solution(mesh):
    in_specs = (
        P(("sp", "tp"), None),
        P(),
        P(None, "tp"),
        P(None, "tp"),
        P(None, "tp"),
        P(None, "tp"),
        P(None, "tp"),
        P("tp"),
        P(),
        P(None, "tp"),
        P(None, "tp"),
        P(None, "tp"),
        P("tp", "sp"),
        P("tp", None, None),
        P("tp", None),
        P("tp", None),
    )
    body = functools.partial(on_device, mesh.shape["sp"], mesh.shape["tp"])
    return jax.shard_map(
        body, mesh=mesh, in_specs=in_specs, out_specs=P(("sp", "tp"), None), check_vma=False
    )
```

time: 266 us -> 102 us (0.38); the launches traced: 262 us -> 101 us
  Pallas kernels: 0 us -> 99.5 us
  matrix products: 82.5 us -> 0 us
  blocking collectives: 53.3 us -> 0 us
  waiting for transfers between devices: 45.6 us -> 0 us
  local copies, waits for them, and re-layouts: 42.4 us -> 1.88 us
  other arithmetic: 22.7 us -> 0 us
  between operations: 14.1 us -> 0.02 us
    pallas_call x0 -> x3, Pallas kernels: none -> 99.5 us  [the longest x1 62.2 us: on_device(): pl.pallas_call(functools.partial(mix_kernel, nsp, heads, rheads), out_sha...]
    dot_general x45 -> x0, matrix products: 82.5 us -> none  [the longest x14 38.8 us: soft_update(): jnp.einsum('hqk,khe->hqe', shifted.astype(jnp.bfloat16), values, preferre...]
    reduce_scatter x1 -> x0, waiting for transfers between devices: 42.7 us -> none  [on_device(): lax.psum_scatter((jnp.dot(diff_out, w_out_diff, preferred_element_type=jn...]
    all_gather x1 -> x0, blocking collectives: 36.4 us -> none  [prefix(): lax.all_gather(a.astype(kind), axis)]
    unnamed x1 -> x0, blocking collectives: 16.8 us -> none
    slice x18 -> x0, local copies, waits for them, and re-layouts: 14.5 us -> none  [the longest x7 7.19 us: attend(): key_block[:, key_width:2 * key_width]]
    cond x42 -> x0, local copies, waits for them, and re-layouts: 9.16 us -> none
    reshape x8 -> x0, local copies, waits for them, and re-layouts: 6.47 us -> none  [the longest x5 4.18 us: split_blocks(): return data.reshape(nblocks, BLOCK, ret_heads, size).transpose(0, 2, 1, 3)]
  transfers between devices with their start and end apart: 3 -> 0, of which waited for: 2 -> 0; matrix products, arithmetic and copies ran while one was open for 18% -> 0% of each run, Pallas kernels for 0% -> 0%
where the time goes in v1:
time: 102 us; the launch traced here: 101 us
  Pallas kernels  99.5 us (98%)
  local copies, waits for them, and re-layouts  1.88 us (2%)
    pallas_call x1, Pallas kernels, on_device(): pl.pallas_call(functools.partial(mix_kernel, nsp, heads, rheads), out_sha...  62.2 us
    pallas_call x1, Pallas kernels, on_device(): pl.pallas_call(functools.partial(merge_kernel, ntp), out_shape=jax.ShapeD...  18.6 us
    pallas_call x1, Pallas kernels, on_device(): pl.pallas_call(functools.partial(project_kernel, ntp, widths), out_shape=...  18.6 us

profile of v1, /device:TPU:24, one launch (start us, length us, event | category | flops | bytes accessed | tf_op | source)
XLA Modules:
  0.0 101.4 jit_solution(10189193875596218115)
XLA Ops:
  0.0 18.6 %project.1 = (bf16[512,256]{1,0:T(8,128)(2,1)}, bf16[512,512]{1,0:T(8,128)(2,1)}, bf16[512,512]{1,0:T(8,128)(2,1)}) custom-call(bf16[128,2048]{1,0:T(8,128)(2,1)} %tokens_ref.1, f32[1,2048]{1,0:T(1,128)} %bitcast.2, bf16[2048,128]{1,0:T(8,128)(2,1)} %refs_0_.1, bf16[2048,128]{1,0:T(8,128)(2,1)} %refs_1_.1, bf16[2048,128]{1,0:T(8,128)(2,1)} %refs_2_.1, ...), custom_call_target="tpu_custom_call" | custom-call | tf_op jit(solution)/shard_map/project/pallas_call | solution.py:436
  18.6 62.2 %mixers.1.mix_ref = bf16[512,512]{1,0:T(8,128)(2,1)} custom-call(f32[2]{0:T(128)} %lam_ref.1, f32[1,128]{1,0:T(1,128)} %bitcast.3, f32[2,512]{1,0:T(2,128)} %log_ref.1, f32[2,64,128]{2,1,0:T(8,128)} %init_ref.1, bf16[512,256]{1,0:T(8,128)(2,1)} %get-tuple-element.8.q_ref, bf16[512,512]{1,0:T(8,128)(2,1)} %get-tuple-element.9.r_ref, ...), custom_call_target="tpu_custom_call" | custom-call | tf_op jit(solution)/shard_map/mixers/pallas_call | solution.py:460
  80.9 18.6 %merge.1 = bf16[128,2048]{1,0:T(8,128)(2,1)} custom-call(bf16[512,512]{1,0:T(8,128)(2,1)} %mixers.1.mix_ref, bf16[256,2048]{1,0:T(8,128)(2,1)} %wd_ref.1, bf16[256,2048]{1,0:T(8,128)(2,1)} %wr_ref.1), custom_call_target="tpu_custom_call" | custom-call | tf_op jit(solution)/shard_map/merge/pallas_call | solution.py:488
  99.5 1.9 %copy.18 = bf16[128,2048]{1,0:T(8,128)(2,1)} copy(bf16[128,2048]{1,0:T(8,128)(2,1)} %merge.1) | data formatting | bytes 1048576

commit v2 on v1

v2 whole, which is shorter than its diff:
```python
import functools

import jax
import jax.numpy as jnp
from jax import lax
from jax.experimental import pallas as pl
from jax.experimental.pallas import tpu as pltpu
from jax.sharding import PartitionSpec as P

BLOCK = 256
NORM_EPS = 1e-06
HEAD_EPS = 1e-05
DIFF_SCALE = 0.8
HIGHEST = lax.Precision.HIGHEST
MESH = pl.DeviceIdType.MESH
F32 = jnp.float32
BF16 = jnp.bfloat16
VMEM_LIMIT = 60 * 1024 * 1024


def remote(src, dst, send, recv, where):
    return pltpu.make_async_remote_copy(
        src_ref=src, dst_ref=dst, send_sem=send, recv_sem=recv,
        device_id=where, device_id_type=MESH,
    )


def head_norm(values):
    return values * lax.rsqrt(jnp.mean(values * values, axis=-1, keepdims=True) + HEAD_EPS)


def nn(a, b, **kw):
    return lax.dot_general(a, b, (((1,), (0,)), ((), ())), preferred_element_type=F32, **kw)


def nt(a, b):
    return lax.dot_general(a, b, (((1,), (1,)), ((), ())), preferred_element_type=F32)


def tn(a, b):
    return lax.dot_general(a, b, (((0,), (0,)), ((), ())), preferred_element_type=F32)


def layer_kernel(nsp, ntp, widths, heads, rheads, lam_ref, tokens_ref, ngain_ref, gain_ref, log_ref,
                 init_ref, *refs):
    nw = len(widths)
    w_refs = refs[:nw]
    wd_ref, wr_ref, out_ref = refs[nw : nw + 3]
    (gat, wbuf, wobuf, kvs, sts, rbuf, qs, peak, den, acc, rmid, upd, mix, mine, sent, from_pair,
     from_chip, wsem, pair_send, cross_send, grecv, sem_z, sem_y, sem_rk, sem_zs, sem_ys, sem_rs,
     mpair_send, mpair_recv, mchip_send, mchip_recv) = refs[nw + 3 :]
    me = lax.axis_index("sp")
    b = lax.rem(me, 2)
    p = me // 2
    npair = nsp // 2
    up = {"sp": lax.rem(me + 2, nsp)}
    side = {"sp": me + 1 - 2 * b}
    tme = lax.axis_index("tp")
    core = lax.rem(tme, 2)
    chip = tme // 2
    nchip = ntp // 2
    tpair = tme + 1 - 2 * core
    pair = {"tp": tpair}
    own_rows = tokens_ref.shape[0]
    rows = own_rows * ntp
    chunk = rows // nchip
    kw = widths[2]
    hd = kw // heads
    val = gain_ref.shape[1]
    first_up = p < npair - 1

    barrier = pltpu.get_barrier_semaphore()

    def greet(where):
        pl.semaphore_signal(barrier, inc=1, device_id=where, device_id_type=MESH)

    greet(side)

    @pl.when(p > 0)
    def _():
        greet({"sp": lax.rem(me + nsp - 2, nsp)})

    @pl.when(first_up)
    def _():
        greet(up)

    greet(pair)
    for d in range(1, nchip):
        greet({"tp": lax.rem(chip + d, nchip) * 2 + core})

    order = (2, 3, 4, 0, 1, 5, 6, 7)
    starts = [sum(widths[:n]) for n in range(nw)]
    loads = {}
    for n in order:
        at = starts[n]
        loads[n] = pltpu.make_async_copy(w_refs[n], wbuf.at[:, at : at + widths[n]], wsem.at[n])
        loads[n].start()
    depth = wd_ref.shape[0]
    out_loads = [
        pltpu.make_async_copy(wd_ref, wobuf.at[:depth], wsem.at[nw]),
        pltpu.make_async_copy(wr_ref, wobuf.at[depth:], wsem.at[nw + 1]),
    ]
    for load in out_loads:
        load.start()
    floats = tokens_ref[...].astype(F32)
    gat[tme] = (
        floats * lax.rsqrt(jnp.mean(floats * floats, axis=-1, keepdims=True) + NORM_EPS) * ngain_ref[...]
    ).astype(BF16)
    pl.semaphore_wait(
        barrier, 1 + nchip + jnp.minimum(p, 1) + jnp.minimum(npair - 1 - p, 1)
    )
    copies = []

    def slab(which, half):
        return gat.at[which, pl.ds(half * (own_rows // 2), own_rows // 2)]

    for d in range(1, nchip):
        there = {"tp": lax.rem(chip + d, nchip) * 2 + core}
        for half in range(2):
            copies.append(remote(slab(tme, half), slab(tme, half), cross_send.at[d, half],
                                 grecv.at[tme, half], there))
            copies[-1].start()

    def to_pair(which, half):
        copies.append(remote(slab(which, half), slab(which, half), pair_send.at[which // 2, half],
                             grecv.at[which, half], pair))
        copies[-1].start()

    def landed(which, half):
        remote(slab(which, half), slab(which, half), pair_send.at[which // 2, half],
               grecv.at[which, half], pair).wait_recv()

    def keys_at(d):
        which = lax.rem(chip + nchip - d, nchip)
        return pl.ds(pl.multiple_of(which * chunk, chunk), chunk)

    def kv_copy(i, j, d, sem, where):
        piece = kvs.at[j, keys_at(d)]
        return remote(piece, piece, sem.at[i, d], sem_rk.at[j, d], where)

    def st_copy(i, j, sem, where):
        return remote(sts.at[j], sts.at[j], sem.at[i], sem_rs.at[j], where)

    qlane = lax.broadcasted_iota(jnp.int32, (chunk, kw), 1)

    def project(d):
        which = lax.rem(chip + nchip - d, nchip)
        both = gat[pl.ds(which * 2, 2)].reshape(chunk, gat.shape[2])
        at = keys_at(d)

        def run(lo, hi, put):
            if d == 0:
                for n in range(lo, hi):
                    loads[n].wait()
            span = sum(widths[lo:hi])
            cut = 256 if span % 256 == 0 else span
            for c in range(0, span, cut):
                put(c, cut, nn(both, wbuf[:, starts[lo] + c : starts[lo] + c + cut]).astype(BF16))

        def put_kv(c, cut, value):
            kvs[me, at, c : c + cut] = value

        def put_r(c, cut, value):
            rbuf[at, c : c + cut] = value

        run(2, 5, put_kv)
        for m in range(2):
            if d == 0:
                loads[m].wait()
            piece = nn(both, wbuf[:, starts[m] : starts[m] + kw]).astype(BF16).astype(F32) * hd ** (-0.5)
            for h in range(heads):
                keep = (qlane >= h * hd) & (qlane < (h + 1) * hd)
                qs[m * heads + h, at, :] = jnp.where(keep, piece, 0.0).astype(BF16)

        @pl.when(first_up)
        def _():
            kv_copy(0, me, d, sem_z, up).start()

        @pl.when(b == 0)
        def _():
            kv_copy(0, me, d, sem_y, side).start()

        run(5, 8, put_r)

    def forward(i, d):
        jz = 2 * (p - i) + b

        @pl.when(i <= p)
        def _():
            kv_copy(i, jz, d, sem_z, up).wait_recv()

            @pl.when(first_up)
            def _():
                kv_copy(i, jz, d, sem_z, up).start()

            kv_copy(i, jz, d, sem_y, side).start()

    for half in range(2):
        to_pair(tme, half)
    for half in range(2):
        landed(tpair, half)
    project(0)
    peak[...] = jnp.full(peak.shape, -jnp.inf, F32)
    den[...] = jnp.zeros(den.shape, F32)
    acc[...] = jnp.zeros(acc.shape, F32)
    forward(1, 0)
    for d in range(1, nchip):
        other = lax.rem(chip + nchip - d, nchip)
        for half in range(2):
            landed(other * 2 + core, half)
            to_pair(other * 2 + core, half)
        for half in range(2):
            landed(other * 2 + 1 - core, half)
        project(d)
    ahead = min(2, npair)
    for i in range(2, ahead + 1):
        forward(i, 0)

    blk = BLOCK
    nblk = rows // blk
    rkw = rheads * hd
    tt = lax.broadcasted_iota(jnp.int32, (blk, blk), 0)
    uu = lax.broadcasted_iota(jnp.int32, (blk, blk), 1)
    lane = lax.broadcasted_iota(jnp.int32, (blk, rkw), 1)
    srow = lax.broadcasted_iota(jnp.int32, (rkw, val), 0)
    decays = []
    span_state = jnp.zeros((rkw, val), F32)
    span_logs = []
    for h in range(rheads):
        ours = (lane >= h * hd) & (lane < (h + 1) * hd)
        keep = (srow >= h * hd) & (srow < (h + 1) * hd)
        state = jnp.zeros((rkw, val), F32)
        log_all = jnp.zeros((1, 1), F32)
        for n in range(nblk):
            at = slice(n * blk, (n + 1) * blk)
            row = log_ref[h : h + 1, at]
            full = jnp.broadcast_to(row, (blk, blk))
            c_col = jnp.sum(jnp.where(uu <= tt, full, 0.0), axis=1, keepdims=True)
            l_col = jnp.sum(jnp.where(uu == tt, full, 0.0), axis=1, keepdims=True)
            c_row = jnp.sum(jnp.where(tt <= uu, l_col, 0.0), axis=0, keepdims=True)
            last = c_col[blk - 1 : blk, :]
            query = jnp.where(ours, rbuf[at, :rkw].astype(F32), 0.0)
            keys = rbuf[at, rkw : 2 * rkw]
            values = rbuf[at, 2 * rkw + h * val : 2 * rkw + (h + 1) * val]
            raw = nt(query.astype(BF16), keys)
            gap = jnp.where(uu <= tt, c_col - c_row, -jnp.inf)
            g = (raw * hd ** (-0.5) * jnp.exp(gap)).astype(BF16)
            rmid[h, at, :] = nn(g, values)
            kd = (keys.astype(F32) * hd ** (-0.5) * jnp.exp(last - c_col)).astype(BF16)
            new = jnp.where(keep, tn(kd, values), 0.0)
            upd[h, n] = new
            state = jnp.exp(last) * state + new
            log_all = log_all + last
            decays.append((c_col, last))
        span_state = span_state + state
        span_logs.append(log_all)
    sts[me, :rkw, :] = span_state.astype(BF16)
    for h in range(rheads):
        wide = jnp.broadcast_to(span_logs[h], (16, val))
        hi = wide.astype(BF16)
        sts[me, rkw + 32 * h : rkw + 32 * h + 16, :] = hi
        sts[me, rkw + 32 * h + 16 : rkw + 32 * h + 32, :] = (wide - hi.astype(F32)).astype(BF16)

    qb = min(rows, 256)

    def attend(j, d):
        diagonal = d is None

        @pl.loop(0, 2 * heads)
        def _(mh):
            m = mh // heads
            h = lax.rem(mh, heads)
            kcol = pl.ds(pl.multiple_of(m * kw, kw), kw)
            vcol = pl.ds(pl.multiple_of(2 * kw + h * val, val), val)
            for n in range(rows // qb):
                at = slice(n * qb, (n + 1) * qb)
                count = (n + 1) * qb if diagonal else chunk
                krows = slice(0, count) if diagonal else keys_at(d)
                scores = nt(qs[mh, at, :], kvs[j, krows, kcol])
                if diagonal:
                    ti = lax.broadcasted_iota(jnp.int32, (qb, count), 0) + n * qb
                    ui = lax.broadcasted_iota(jnp.int32, (qb, count), 1)
                    scores = jnp.where(ui <= ti, scores, -jnp.inf)
                old = peak[mh, at, :]
                top = jnp.maximum(old, jnp.max(scores, axis=1, keepdims=True))
                e = jnp.exp(scores - top[:, :1])
                part = e[:, :128]
                for c in range(128, count, 128):
                    part = part + e[:, c : c + 128]
                weighted = nn(e.astype(BF16), kvs[j, krows, vcol])
                rescale = jnp.exp(old - top)
                peak[mh, at, :] = top
                den[mh, at, :] = den[mh, at, :] * rescale + part
                acc[mh, at, :] = acc[mh, at, :] * rescale[:, :1] + weighted

    attend(me, None)

    @pl.when(first_up)
    def _():
        st_copy(0, me, sem_zs, up).start()

    @pl.when(b == 0)
    def _():
        st_copy(0, me, sem_ys, side).start()

    for d in range(nchip):
        @pl.loop(1, npair + 1)
        def _(i):
            jz = 2 * (p - i) + b
            jy = 2 * (p - i + 1) + 1 - b
            if d == 0:
                @pl.when(i > ahead)
                def _():
                    forward(i, 0)
            else:
                forward(i, d)

            @pl.when(i <= p)
            def _():
                if d == nchip - 1:
                    st_copy(i, jz, sem_zs, up).wait_recv()

                    @pl.when(first_up)
                    def _():
                        st_copy(i, jz, sem_zs, up).start()

                    st_copy(i, jz, sem_ys, side).start()
                attend(jz, d)

            @pl.when((i - 1 <= p) & ((b == 1) | (i > 1)))
            def _():
                kv_copy(i, jy, d, sem_y, side).wait_recv()
                if d == nchip - 1:
                    st_copy(i, jy, sem_ys, side).wait_recv()
                attend(jy, d)

    first = []
    for h in range(rheads):
        parts = [jnp.zeros((hd, val), F32)] * h + [init_ref[h]] + [jnp.zeros((hd, val), F32)] * (rheads - 1 - h)
        first.append(jnp.concatenate(parts, axis=0) if rheads > 1 else parts[0])

    def join(j, states):
        out = []
        for h in range(rheads):
            keep = (srow >= h * hd) & (srow < (h + 1) * hd)
            base = rkw + 32 * h
            log = sts[j, base : base + 16, :].astype(F32) + sts[j, base + 16 : base + 32, :].astype(F32)
            piece = jnp.where(keep, sts[j, :rkw, :].astype(F32), 0.0)
            out.append(jnp.exp(log[:1, :]) * states[h] + piece)
        return tuple(out)

    carried = lax.fori_loop(0, me, join, tuple(first))
    for h in range(rheads):
        state = carried[h]
        for n in range(nblk):
            at = slice(n * blk, (n + 1) * blk)
            c_col, last = decays[h * nblk + n]
            query = rbuf[at, :rkw].astype(F32) * jnp.exp(c_col)
            result = rmid[h, at, :] + nn(query, state, precision=HIGHEST)
            if n + 1 < nblk:
                state = jnp.exp(last) * state + upd[h, n]
            mix[at, heads * val + h * val : heads * val + (h + 1) * val] = head_norm(result).astype(BF16)
    for h in range(heads):
        pieces = []
        for m in range(2):
            mh = m * heads + h
            total = jnp.sum(den[mh], axis=1, keepdims=True)
            pieces.append(acc[mh] / total)
        mixed = pieces[0] - lam_ref[h] * pieces[1]
        mix[:, h * val : (h + 1) * val] = (head_norm(mixed) * gain_ref[...] * DIFF_SCALE).astype(BF16)
    for load in out_loads:
        load.wait()

    width = out_ref.shape[1]
    cut = mine.shape[2]
    npiece = width // cut

    def partial(owner, n):
        part = mix[pl.ds(pl.multiple_of(owner * own_rows, own_rows), own_rows), :]
        return nn(part, wobuf[:, n * cut : (n + 1) * cut])

    def pair_copy(d, n):
        return remote(mine.at[d * npiece + n], from_pair.at[d * npiece + n], mpair_send.at[d, n],
                      mpair_recv.at[d, n], pair)

    def chip_copy(d, n):
        there = lax.rem(chip + d, nchip) * 2 + core
        return remote(sent.at[d * npiece + n], from_chip.at[d * npiece + n], mchip_send.at[d, n],
                      mchip_recv.at[d, n], {"tp": there})

    targets = list(range(1, nchip)) + [0]
    for d in targets:
        target = lax.rem(chip + d, nchip) * 2
        for n in range(npiece):
            mine[d * npiece + n] = partial(target + 1 - core, n).astype(BF16)
            pair_copy(d, n).start()
        if d:
            for n in range(npiece):
                ours = partial(target + core, n)
                pair_copy(d, n).wait_recv()
                sent[d * npiece + n] = (ours + from_pair[d * npiece + n].astype(F32)).astype(BF16)
                chip_copy(d, n).start()
    for n in range(npiece):
        total = partial(tme, n)
        pair_copy(0, n).wait_recv()
        total = total + from_pair[n].astype(F32)
        for d in range(1, nchip):
            chip_copy(d, n).wait_recv()
            total = total + from_chip[d * npiece + n].astype(F32)
        out_ref[:, n * cut : (n + 1) * cut] = total.astype(BF16)

    for copy in copies:
        copy.wait_send()

    @pl.loop(0, npair)
    def _(i):
        j = 2 * (p - i) + b

        @pl.when((i <= p) & first_up)
        def _():
            for d in range(nchip):
                kv_copy(i, j, d, sem_z, up).wait_send()
            st_copy(i, j, sem_zs, up).wait_send()

        @pl.when((i <= p) & ((i > 0) | (b == 0)))
        def _():
            for d in range(nchip):
                kv_copy(i, j, d, sem_y, side).wait_send()
            st_copy(i, j, sem_ys, side).wait_send()

    for d in targets:
        for n in range(npiece):
            pair_copy(d, n).wait_send()
            if d:
                chip_copy(d, n).wait_send()


VMEM = pl.BlockSpec(memory_space=pltpu.VMEM)
ANY = pl.BlockSpec(memory_space=pl.ANY)
SMEM = pl.BlockSpec(memory_space=pltpu.SMEM)
DMA = pltpu.SemaphoreType.DMA


def params(number):
    return pltpu.CompilerParams(
        collective_id=number, has_side_effects=True, vmem_limit_bytes=VMEM_LIMIT
    )


def on_device(nsp, ntp, tokens, norm_gain, w_query_one, w_query_two, w_key_one, w_key_two, w_value,
              mix_lambda, head_gain, w_ret_query, w_ret_key, w_ret_value, retain_log, init_state,
              w_out_diff, w_out_ret):
    weights = (w_query_one, w_query_two, w_key_one, w_key_two, w_value, w_ret_query, w_ret_key, w_ret_value)
    widths = tuple(w.shape[1] for w in weights)
    own_rows, model = tokens.shape
    rows = own_rows * ntp
    nchip = ntp // 2
    npair = nsp // 2
    heads = mix_lambda.shape[0]
    rheads, hd, val = init_state.shape
    kw = widths[2]
    width = w_out_diff.shape[1]
    npiece = 4
    cut = width // npiece
    return pl.pallas_call(
        functools.partial(layer_kernel, nsp, ntp, widths, heads, rheads),
        out_shape=jax.ShapeDtypeStruct((own_rows, width), BF16),
        in_specs=[SMEM] + [VMEM] * 5 + [ANY] * (len(weights) + 2),
        out_specs=VMEM,
        scratch_shapes=[
            pltpu.VMEM((ntp, own_rows, model), BF16),
            pltpu.VMEM((model, sum(widths)), BF16),
            pltpu.VMEM((w_out_diff.shape[0] + w_out_ret.shape[0], width), BF16),
            pltpu.VMEM((nsp, rows, sum(widths[2:5])), BF16),
            pltpu.VMEM((nsp, rheads * hd + 32 * rheads, val), BF16),
            pltpu.VMEM((rows, sum(widths[5:])), BF16),
            pltpu.VMEM((2 * heads, rows, kw), BF16),
            pltpu.VMEM((2 * heads, rows, 128), F32),
            pltpu.VMEM((2 * heads, rows, 128), F32),
            pltpu.VMEM((2 * heads, rows, val), F32),
            pltpu.VMEM((rheads, rows, val), F32),
            pltpu.VMEM((rheads, rows // BLOCK, rheads * hd, val), F32),
            pltpu.VMEM((rows, (heads + rheads) * val), BF16),
            pltpu.VMEM((nchip * npiece, own_rows, cut), BF16),
            pltpu.VMEM((nchip * npiece, own_rows, cut), BF16),
            pltpu.VMEM((nchip * npiece, own_rows, cut), BF16),
            pltpu.VMEM((nchip * npiece, own_rows, cut), BF16),
            DMA((len(weights) + 2,)),
            DMA((nchip, 2)),
            DMA((nchip, 2)),
            DMA((ntp, 2)),
            DMA((npair + 1, nchip)),
            DMA((npair + 1, nchip)),
            DMA((nsp, nchip)),
            DMA((npair + 1,)),
            DMA((npair + 1,)),
            DMA((nsp,)),
            DMA((nchip, npiece)),
            DMA((nchip, npiece)),
            DMA((nchip, npiece)),
            DMA((nchip, npiece)),
        ],
        compiler_params=params(0),
        name="layer",
    )(mix_lambda, tokens, norm_gain[None, :], head_gain[None, :], retain_log, init_state, *weights,
      w_out_diff, w_out_ret)


def solution(mesh):
    in_specs = (
        P(("sp", "tp"), None),
        P(),
        P(None, "tp"),
        P(None, "tp"),
        P(None, "tp"),
        P(None, "tp"),
        P(None, "tp"),
        P("tp"),
        P(),
        P(None, "tp"),
        P(None, "tp"),
        P(None, "tp"),
        P("tp", "sp"),
        P("tp", None, None),
        P("tp", None),
        P("tp", None),
    )
    body = functools.partial(on_device, mesh.shape["sp"], mesh.shape["tp"])
    return jax.shard_map(
        body, mesh=mesh, in_specs=in_specs, out_specs=P(("sp", "tp"), None), check_vma=False
    )
```

time: 102 us -> 99 us (0.971)
  Pallas kernels: 99.5 us -> 96.8 us
    pallas_call x3 -> x1, Pallas kernels: 99.5 us -> 96.8 us  [on_device(): pl.pallas_call(functools.partial(layer_kernel, nsp, ntp, widths, heads, r...]
where the time goes in v2:
time: 99 us; the launch traced here: 98.7 us
  Pallas kernels  96.8 us (98%)
  local copies, waits for them, and re-layouts  1.88 us (2%)
    pallas_call x1, Pallas kernels, on_device(): pl.pallas_call(functools.partial(layer_kernel, nsp, ntp, widths, heads, r...  96.8 us

profile of v2, /device:TPU:24, one launch (start us, length us, event | category | flops | bytes accessed | tf_op | source)
XLA Modules:
  0.0 98.7 jit_solution(12703196225193955652)
XLA Ops:
  0.0 96.8 %layer.1 = bf16[128,2048]{1,0:T(8,128)(2,1)} custom-call(f32[2]{0:T(128)} %lam_ref.1, bf16[128,2048]{1,0:T(8,128)(2,1)} %tokens_ref.1, f32[1,2048]{1,0:T(1,128)} %bitcast.2, f32[1,128]{1,0:T(1,128)} %bitcast.3, f32[2,512]{1,0:T(2,128)} %log_ref.1, f32[2,64,128]{2,1,0:T(8,128)} %init_ref.1, bf16[2048,128]{1,0:T(8,128)(2,1)} %refs_0_.1, ...), custom_call_target="tpu_custom_call" | custom-call | tf_op jit(solution)/shard_map/layer/pallas_call | solution.py:465
  96.8 1.9 %copy.18 = bf16[128,2048]{1,0:T(8,128)(2,1)} copy(bf16[128,2048]{1,0:T(8,128)(2,1)} %layer.1) | data formatting | bytes 1048576

commit v3 on v2

--- a/solution.py
+++ b/solution.py
@@ -212,9 +212,8 @@
         for half in range(2):
             landed(other * 2 + 1 - core, half)
         project(d)
-    ahead = min(2, npair)
-    for i in range(2, ahead + 1):
-        forward(i, 0)
+    if npair > 1:
+        forward(2, 0)
 
     blk = BLOCK
     nblk = rows // blk
@@ -263,8 +262,7 @@
 
     qb = min(rows, 256)
 
-    def attend(j, d):
-        diagonal = d is None
+    def attend(j, diagonal):
 
         @pl.loop(0, 2 * heads)
         def _(mh):
@@ -274,8 +272,8 @@
             vcol = pl.ds(pl.multiple_of(2 * kw + h * val, val), val)
             for n in range(rows // qb):
                 at = slice(n * qb, (n + 1) * qb)
-                count = (n + 1) * qb if diagonal else chunk
-                krows = slice(0, count) if diagonal else keys_at(d)
+                count = (n + 1) * qb if diagonal else rows
+                krows = slice(0, count)
                 scores = nt(qs[mh, at, :], kvs[j, krows, kcol])
                 if diagonal:
                     ti = lax.broadcasted_iota(jnp.int32, (qb, count), 0) + n * qb
@@ -293,7 +291,11 @@
                 den[mh, at, :] = den[mh, at, :] * rescale + part
                 acc[mh, at, :] = acc[mh, at, :] * rescale[:, :1] + weighted
 
-    attend(me, None)
+    @pl.loop(3, npair + 1)
+    def _(i):
+        forward(i, 0)
+
+    attend(me, True)
 
     @pl.when(first_up)
     def _():
@@ -303,36 +305,30 @@
     def _():
         st_copy(0, me, sem_ys, side).start()
 
-    for d in range(nchip):
-        @pl.loop(1, npair + 1)
-        def _(i):
-            jz = 2 * (p - i) + b
-            jy = 2 * (p - i + 1) + 1 - b
-            if d == 0:
-                @pl.when(i > ahead)
-                def _():
-                    forward(i, 0)
-            else:
-                forward(i, d)
-
-            @pl.when(i <= p)
+    @pl.loop(1, npair + 1)
+    def _(i):
+        jz = 2 * (p - i) + b
+        jy = 2 * (p - i + 1) + 1 - b
+        for d in range(1, nchip):
+            forward(i, d)
+
+        @pl.when(i <= p)
+        def _():
+            st_copy(i, jz, sem_zs, up).wait_recv()
+
+            @pl.when(first_up)
             def _():
-                if d == nchip - 1:
-                    st_copy(i, jz, sem_zs, up).wait_recv()
-
-                    @pl.when(first_up)
-                    def _():
-                        st_copy(i, jz, sem_zs, up).start()
-
-                    st_copy(i, jz, sem_ys, side).start()
-                attend(jz, d)
-
-            @pl.when((i - 1 <= p) & ((b == 1) | (i > 1)))
-            def _():
+                st_copy(i, jz, sem_zs, up).start()
+
+            st_copy(i, jz, sem_ys, side).start()
+            attend(jz, False)
+
+        @pl.when((i - 1 <= p) & ((b == 1) | (i > 1)))
+        def _():
+            for d in range(nchip):
                 kv_copy(i, jy, d, sem_y, side).wait_recv()
-                if d == nchip - 1:
-                    st_copy(i, jy, sem_ys, side).wait_recv()
-                attend(jy, d)
+            st_copy(i, jy, sem_ys, side).wait_recv()
+            attend(jy, False)
 
     first = []
     for h in range(rheads):

time: 99 us -> 85.3 us (0.86)
  Pallas kernels: 96.8 us -> 82.7 us
    pallas_call x1, Pallas kernels: 96.8 us -> 82.7 us  [on_device(): pl.pallas_call(functools.partial(layer_kernel, nsp, ntp, widths, heads, r...]
where the time goes in v3:
time: 85.3 us; the launch traced here: 84.6 us
  Pallas kernels  82.7 us (97%)
  local copies, waits for them, and re-layouts  1.88 us (2%)
    pallas_call x1, Pallas kernels, on_device(): pl.pallas_call(functools.partial(layer_kernel, nsp, ntp, widths, heads, r...  82.7 us
    unnamed x1, local copies, waits for them, and re-layouts  1.88 us

profile of v3, /device:TPU:24, one launch (start us, length us, event | category | flops | bytes accessed | tf_op | source)
XLA Modules:
  0.0 84.6 jit_solution(10773345378971208054)
XLA Ops:
  0.0 82.7 %layer.1 = bf16[128,2048]{1,0:T(8,128)(2,1)} custom-call(f32[2]{0:T(128)} %lam_ref.1, bf16[128,2048]{1,0:T(8,128)(2,1)} %tokens_ref.1, f32[1,2048]{1,0:T(1,128)} %bitcast.2, f32[1,128]{1,0:T(1,128)} %bitcast.3, f32[2,512]{1,0:T(2,128)} %log_ref.1, f32[2,64,128]{2,1,0:T(8,128)} %init_ref.1, bf16[2048,128]{1,0:T(8,128)(2,1)} %refs_0_.1, ...), custom_call_target="tpu_custom_call" | custom-call | tf_op jit(solution)/shard_map/layer/pallas_call | solution.py:461
  82.7 1.9 %copy.18 = bf16[128,2048]{1,0:T(8,128)(2,1)} copy(bf16[128,2048]{1,0:T(8,128)(2,1)} %layer.1) | data formatting | bytes 1048576
